TPU v7x, 32 devices: a whole 2x2x4 slice. The times are simulated.
32 devices in a mesh: sp: 8 (over z, y), tp: 4 (over x, core).
Axes of the slice: x: 2, y: 2, z: 4, core: 2. Of those that a mesh axis runs over, the one named last changes fastest.
Arguments:
- layer_input: bfloat16 [8, 1024, 2048], P(None, ('sp', 'tp')), may hold values from -6 to 6
- input_gain: float32 [2048], replicated, may hold values from 0.5 to 1.5
- narrowing_matrix: bfloat16 [2048, 512], replicated, may hold values from -0.125 to 0.125
- rotary_down: bfloat16 [2048, 64], replicated, may hold values from -0.125 to 0.125
- summary_scaling: float32 [512], replicated, may hold values from 0.5 to 1.5
- lookup_widening: bfloat16 [512, 16, 128], P('tp'), may hold values from -0.25 to 0.25
- payload_widening: bfloat16 [512, 16, 128], P('tp'), may hold values from -0.25 to 0.25
- query_nope: bfloat16 [8, 16, 128], P('sp', 'tp'), may hold values from -6 to 6
- query_rotary: bfloat16 [8, 16, 64], P('sp', 'tp'), may hold values from -6 to 6
Outputs:
- stored_summaries: bfloat16 [8, 1024, 512], P('sp', None, 'tp')
- rotary_cache: bfloat16 [8, 1024, 64], P('sp', None, 'tp')
- first_read: bfloat16 [8, 16, 128], P('sp', 'tp')
All inputs are finite; a program needn't handle non-finite values.
Results may differ from a plain program's by a relative error of at most 0.02.
Values may be sent and summed in bfloat16 or wider, within the bound.
A program may use at most 64 MiB of HBM per device.

v0:
```python
import jax
import jax.numpy as jnp
from jax import lax
from jax.sharding import PartitionSpec as P

QK_ROPE = 64
PLAIN_MATCH_SPAN = 128
norm_eps = 1e-06
rotary_base = 10000.0


def summed_rows(portion, width, axis):
    count = width * lax.axis_size(axis)
    return lax.psum_scatter(portion(jnp.int32(0), count), axis, scatter_dimension=0, tiled=True)


def rescaled_lines(vector):
    return vector * lax.rsqrt(jnp.mean(vector * vector, axis=-1, keepdims=True) + norm_eps)


def rotate(vector, position):
    half_width = vector.shape[-1] // 2
    frequency = 1.0 / rotary_base ** (
        jnp.arange(half_width, dtype=jnp.float32) * 2.0 / vector.shape[-1]
    )
    angles = position * frequency
    first_half = vector[..., :half_width]
    second_half = vector[..., half_width:]
    return jnp.concatenate(
        [
            first_half * jnp.cos(angles) - second_half * jnp.sin(angles),
            second_half * jnp.cos(angles) + first_half * jnp.sin(angles),
        ],
        axis=-1,
    )


def to_pieces(array, sp_count, tp_count):
    seq_count, pos_local, cache_width = array.shape
    seq_each = seq_count // sp_count
    width_each = cache_width // tp_count
    array = array.reshape(sp_count, seq_each, pos_local, tp_count, width_each)
    array = array.transpose(0, 3, 1, 2, 4)
    return array.reshape(sp_count * tp_count, seq_each, pos_local, width_each)


def shards(
    layer_input,
    input_gain,
    narrowing_matrix,
    rotary_down,
    summary_scaling,
    lookup_widening,
    payload_widening,
    query_nope,
    query_rotary,
):
    seq_count, pos_local, feature_width = layer_input.shape
    sp_count = lax.axis_size("sp")
    tp_count = lax.axis_size("tp")
    block_index = lax.axis_index(("sp", "tp"))
    normed = (rescaled_lines(layer_input.astype(jnp.float32)) * input_gain).astype(jnp.bfloat16)
    flat_rows = normed.reshape(seq_count * pos_local, feature_width)
    hidden_summary = jnp.dot(
        flat_rows, narrowing_matrix, preferred_element_type=jnp.float32
    ).astype(jnp.bfloat16)
    rotary = jnp.dot(flat_rows, rotary_down, preferred_element_type=jnp.float32).astype(
        jnp.bfloat16
    )
    hidden_summary = (
        (rescaled_lines(hidden_summary.astype(jnp.float32)) * summary_scaling)
        .astype(jnp.bfloat16)
        .reshape(seq_count, pos_local, -1)
    )
    positions = (block_index * pos_local + jnp.arange(pos_local, dtype=jnp.int32)).astype(
        jnp.float32
    )[None, :, None]
    rotary = rotate(rotary.astype(jnp.float32).reshape(seq_count, pos_local, -1), positions).astype(
        jnp.bfloat16
    )
    moved = (
        lax.all_to_all(
            to_pieces(hidden_summary, sp_count, tp_count),
            ("sp", "tp"),
            split_axis=0,
            concat_axis=2,
            tiled=True,
        ),
        lax.all_to_all(
            to_pieces(rotary, sp_count, tp_count),
            ("sp", "tp"),
            split_axis=0,
            concat_axis=2,
            tiled=True,
        ),
    )
    hidden_summary = moved[0][0]
    rotary = moved[1][0]
    pos_total = hidden_summary.shape[1]
    rot_each = rotary.shape[2]
    head_each = query_nope.shape[1]
    query_all, turn_all = (
        lax.all_gather(query_nope, "tp", axis=1, tiled=True),
        lax.all_gather(query_rotary, "tp", axis=1, tiled=True),
    )
    absorbed = jnp.einsum(
        "shd,chd->shc", query_all, lookup_widening, preferred_element_type=jnp.float32
    ).astype(jnp.bfloat16)
    query_turned = rotate(turn_all.astype(jnp.float32), jnp.float32(pos_total)).astype(jnp.bfloat16)
    turned_mine = lax.dynamic_slice_in_dim(
        query_turned, lax.axis_index("tp") * rot_each, rot_each, 2
    )
    score_scale = (PLAIN_MATCH_SPAN + QK_ROPE) ** (-0.5)
    partial_value = (
        jnp.einsum("shc,spc->shp", absorbed, hidden_summary, preferred_element_type=jnp.float32)
        + jnp.einsum("shr,spr->shp", turned_mine, rotary, preferred_element_type=jnp.float32)
    ) * score_scale
    scores = lax.psum(partial_value.astype(jnp.bfloat16), "tp").astype(jnp.float32)
    attention = jax.nn.softmax(scores, axis=-1).astype(jnp.bfloat16)
    context = jnp.einsum(
        "shp,spc->shc", attention, hidden_summary, preferred_element_type=jnp.float32
    ).astype(jnp.bfloat16)

    def project_heads(row_start, row_count):
        part_context = lax.dynamic_slice_in_dim(context, row_start, row_count, 1)
        part_weight = lax.dynamic_slice_in_dim(payload_widening, row_start, row_count, 1)
        return jnp.einsum(
            "shc,chv->hsv", part_context, part_weight, preferred_element_type=jnp.float32
        )

    values = summed_rows(project_heads, head_each, "tp")
    first_read = rescaled_lines(values.transpose(1, 0, 2)).astype(jnp.bfloat16)
    return (hidden_summary, rotary, first_read)


def solution(mesh):
    return jax.shard_map(
        shards,
        mesh=mesh,
        in_specs=(
            P(None, ("sp", "tp"), None),
            P(),
            P(),
            P(),
            P(),
            P("tp", None, None),
            P("tp", None, None),
            P("sp", "tp", None),
            P("sp", "tp", None),
        ),
        out_specs=(P("sp", None, "tp"), P("sp", None, "tp"), P("sp", "tp", None)),
        check_vma=False,
    )
```

profile of v0, /device:TPU:0, one launch (start us, length us, event | category | flops | bytes accessed | tf_op | source)
XLA Modules:
  0.0 55.6 jit_solution(11520406021461989264)
XLA Ops:
  0.7 1.7 %fusion = f32[8,32]{1,0:T(8,128)S(1)} fusion(bf16[8,32,2048]{2,1,0:T(8,128)(2,1)} %param.9), kind=kLoop, calls=%fused_computation.2 | loop fusion | flops 1572608 | bytes 1049600 | tf_op jit(solution)/shard_map/reduce_sum | solution.py:18
  2.4 1.5 %fusion.2 = bf16[8,32,2048]{2,1,0:T(8,128)(2,1)S(1)} fusion(bf16[8,32,2048]{2,1,0:T(8,128)(2,1)} %param.9, f32[2048]{0:T(1024)} %param.10, f32[8,32]{1,0:T(8,128)S(1)} %add_rsqrt_fusion), kind=kLoop, calls=%fused_computation.4 | loop fusion | flops 2097152 | bytes 2106368 | tf_op jit(solution)/shard_map/convert_element_type | solution.py:62
  4.0 0.4 fusion.6
  5.0 0.8 %reshape.300 = bf16[32,2,256]{2,1,0:T(2,128)(2,1)} reshape(bf16[32,1,16,32]{3,2,1,0:T(8,128)(2,1)S(1)} %bitcast.62) | data formatting | bytes 65536
  5.8 7.3 %all-to-all-start.1 = ((bf16[32,2,256]{2,1,0:T(2,128)(2,1)}), bf16[32,2,256]{2,1,0:T(2,128)(2,1)S(1)}, u32[]{:S(2)}, u32[]{:S(2)}) async-start(bf16[32,2,256]{2,1,0:T(2,128)(2,1)} %reshape.300), calls=%async_computation.1 | async-start | bytes 65536 | tf_op jit(solution)/shard_map/all_to_all | solution.py:89
  13.1 5.2 %all_gather.7 = bf16[1,16,64]{2,0,1:T(2,128)(2,1)S(1)} all-gather(bf16[1,4,64]{2,0,1:T(2,128)(2,1)S(1)} %copy.37), channel_id=1, replica_groups=mesh['sp'=8,'tp'=4] {'tp'}, dimensions={1}, use_global_device_ids=true | all-gather | bytes 2560 | tf_op jit(solution)/shard_map/all_gather | solution.py:104
  18.3 0.8 %multiply_reduce_fusion = (f32[256]{0:T(256)S(1)}, f32[256,512]{1,0:T(8,128)S(1)}) fusion(bf16[256,2048]{1,0:T(8,128)(2,1)S(1)} %bitcast.57, bf16[2048,512]{1,0:T(8,128)(2,1)S(1)} %copy-done), kind=kOutput, calls=%fused_computation.20 | convolution fusion | flops 537394944 | bytes 3671040 | tf_op jit(solution)/shard_map/dot_general | solution.py:64
  19.4 0.8 %copy.31 = bf16[8,1,32,4,128]{4,2,3,0,1:T(8,128)(2,1)} copy(bf16[8,1,32,4,128]{4,3,2,0,1:T(4,128)(2,1)S(1)} %reshape_reshape.3) | data formatting | bytes 524288 | tf_op jit(solution)/shard_map/reshape;reshape | solution.py:42
  20.1 0.2 all-to-all-done.1
  20.4 5.6 %all-to-all-start = ((bf16[32,1,32,128]{3,2,1,0:T(8,128)(2,1)}), bf16[32,1,32,128]{3,2,1,0:T(8,128)(2,1)S(1)}, u32[]{:S(2)}, u32[]{:S(2)}) async-start(bf16[32,1,32,128]{3,2,1,0:T(8,128)(2,1)} %bitcast.3), calls=%async_computation | async-start | bytes 524288 | tf_op jit(solution)/shard_map/all_to_all | solution.py:82
  26.1 0.6 %dynamic-slice = u32[1]{0:T(128)} dynamic-slice(u32[32]{0:T(128)S(1)} %copy-done.7, u32[]{:T(128)S(6)} %add.73), dynamic_slice_sizes={1} | dynamic-slice | bytes 12
  27.3 5.2 %all_gather.6 = bf16[1,16,128]{2,0,1:T(2,128)(2,1)S(1)} all-gather(bf16[1,4,128]{2,0,1:T(2,128)(2,1)S(1)} %copy.36), channel_id=1, replica_groups=mesh['sp'=8,'tp'=4] {'tp'}, dimensions={1}, use_global_device_ids=true | all-gather | bytes 5120 | tf_op jit(solution)/shard_map/all_gather | solution.py:103
  32.6 0.4 fusion.11
  33.2 0.2 reshape.287
  33.3 0.8 %squeeze.7 = bf16[1,1024,16]{1,2,0:T(8,128)(2,1)} reshape(bf16[32,1,32,16]{2,0,3,1:T(8,128)(2,1)S(1)} %copy.35) | data formatting | bytes 65536 | tf_op jit(solution)/shard_map/squeeze | solution.py:98
  34.1 2.4 %all-to-all-done = bf16[32,1,32,128]{3,2,1,0:T(8,128)(2,1)S(1)} async-done(((bf16[32,1,32,128]{3,2,1,0:T(8,128)(2,1)}), bf16[32,1,32,128]{3,2,1,0:T(8,128)(2,1)S(1)}, u32[]{:S(2)}, u32[]{:S(2)}) %all-to-all-start) | async-done | bytes 262176 | tf_op jit(solution)/shard_map/all_to_all | solution.py:82
  36.7 0.2 fusion.7
  36.9 10.6 %psum.7 = bf16[1,16,1024]{2,1,0:T(8,128)(2,1)S(1)} all-reduce(bf16[1,16,1024]{2,1,0:T(8,128)(2,1)S(1)} %fusion.7), channel_id=1, replica_groups=mesh['sp'=8,'tp'=4] {'tp'}, use_global_device_ids=true, to_apply=%region_2.0 | all-reduce | flops 16384 | bytes 65536 | tf_op jit(solution)/shard_map/psum | solution.py:118
  47.7 0.2 fusion.13
  47.9 0.2 fusion.8
  48.1 0.3 fusion.9
  48.3 5.8 %all-reduce = f32[16,1,128]{2,0,1:T(8,128)S(1)} all-reduce(f32[16,1,128]{2,0,1:T(8,128)S(1)} %bitcast.64), channel_id=2, replica_groups=mesh['sp'=8,'tp'=4] {'tp'}, use_global_device_ids=true, to_apply=%region_5.0.clone | all-reduce | flops 2048 | bytes 16384
  54.2 0.6 %multiply_convert_fusion.1 = bf16[1,4,128]{2,1,0:T(4,128)(2,1)} fusion(f32[16,1,128]{2,0,1:T(8,128)S(1)} %all-reduce, u32[]{:T(128)S(6)} %multiply.33, f32[4]{0:T(128)S(1)} %add_rsqrt_fusion.2), kind=kLoop, calls=%fused_computation.46 | loop fusion | flops 1024 | bytes 3092 | tf_op jit(solution)/shard_map/convert_element_type | solution.py:132
  54.9 0.7 %copy.56 = bf16[1,1024,128]{2,1,0:T(8,128)(2,1)} copy(bf16[1,1024,128]{2,1,0:T(8,128)(2,1)S(1)} %bitcast.60) | data formatting | bytes 524288
  (39 shorter events, 1.6 us)
Async XLA Ops:
  0.6 17.7 %copy-start = (bf16[2048,512]{1,0:T(8,128)(2,1)S(1)}, bf16[2048,512]{1,0:T(8,128)(2,1)}, u32[]{:S(2)}) copy-start(bf16[2048,512]{1,0:T(8,128)(2,1)} %param.11) | copy-start | bytes 6291460
  0.6 3.3 %copy-start.1 = (bf16[2048,64]{0,1:T(8,128)(2,1)S(1)}, bf16[2048,64]{0,1:T(8,128)(2,1)}, u32[]{:S(2)}) copy-start(bf16[2048,64]{0,1:T(8,128)(2,1)} %param.12) | copy-start | bytes 786436
  2.4 10.7 %copy-start.3 = (bf16[1,4,64]{2,1,0:T(4,128)(2,1)S(1)}, bf16[1,4,64]{2,1,0:T(4,128)(2,1)}, u32[]{:S(2)}) copy-start(bf16[1,4,64]{2,1,0:T(4,128)(2,1)} %param.17) | copy-start | bytes 1540
  5.0 14.2 %copy-start.2 = (f32[512]{0:T(512)S(1)}, f32[512]{0:T(512)}, u32[]{:S(2)}) copy-start(f32[512]{0:T(512)} %param.13) | copy-start | bytes 6148
  5.8 14.6 %all-to-all-start.1 = ((bf16[32,2,256]{2,1,0:T(2,128)(2,1)}), bf16[32,2,256]{2,1,0:T(2,128)(2,1)S(1)}, u32[]{:S(2)}, u32[]{:S(2)}) async-start(bf16[32,2,256]{2,1,0:T(2,128)(2,1)} %reshape.300), calls=%async_computation.1 | async-start | bytes 65536 | tf_op jit(solution)/shard_map/all_to_all | solution.py:89
  19.1 6.9 %copy-start.4 = (bf16[1,4,128]{2,1,0:T(4,128)(2,1)S(1)}, bf16[1,4,128]{2,1,0:T(4,128)(2,1)}, u32[]{:S(2)}) copy-start(bf16[1,4,128]{2,1,0:T(4,128)(2,1)} %param.16) | copy-start | bytes 3076
  19.1 7.0 %copy-start.7 = (u32[32]{0:T(128)S(1)}, u32[32]{0:T(128)}, u32[]{:S(2)}) copy-start(u32[32]{0:T(128)} %constant.54) | copy-start | bytes 388
  19.1 13.5 %copy-start.5 = (bf16[128,16,128]{2,1,0:T(8,128)(2,1)S(1)}, bf16[128,16,128]{2,1,0:T(8,128)(2,1)}, u32[]{:S(2)}) copy-start(bf16[128,16,128]{2,1,0:T(8,128)(2,1)} %param.14) | copy-start | bytes 1572868
  19.4 28.7 %copy-start.6 = (bf16[128,16,128]{2,1,0:T(8,128)(2,1)S(1)}, bf16[128,16,128]{2,1,0:T(8,128)(2,1)}, u32[]{:S(2)}) copy-start(bf16[128,16,128]{2,1,0:T(8,128)(2,1)} %param.15) | copy-start | bytes 1572868
  20.4 16.2 %all-to-all-start = ((bf16[32,1,32,128]{3,2,1,0:T(8,128)(2,1)}), bf16[32,1,32,128]{3,2,1,0:T(8,128)(2,1)S(1)}, u32[]{:S(2)}, u32[]{:S(2)}) async-start(bf16[32,1,32,128]{3,2,1,0:T(8,128)(2,1)} %bitcast.3), calls=%async_computation | async-start | bytes 524288 | tf_op jit(solution)/shard_map/all_to_all | solution.py:82
where the time goes:
time: 55.9 us; the launch traced here: 55.6 us
  blocking collectives  26.7 us (48%)
  starting transfers between devices  12.9 us (23%)
  other arithmetic  4.95 us (9%)
  local copies, waits for them, and re-layouts  4.3 us (8%)
  waiting for transfers between devices  2.64 us (5%)
  matrix products  2.46 us (4%)
  between operations  1.56 us (3%)
    psum x1, blocking collectives, shards(): lax.psum(partial_value.astype(jnp.bfloat16), 'tp').astype(jnp.float32)  10.6 us
    all_to_all x1, starting transfers between devices, shards(): lax.all_to_all(to_pieces(rotary, sp_count, tp_count), ('sp', 'tp'), split...  7.33 us
    unnamed x1, blocking collectives  5.76 us
    all_to_all x1, starting transfers between devices, shards(): lax.all_to_all(to_pieces(hidden_summary, sp_count, tp_count), ('sp', 'tp'...  5.61 us
    all_gather x1, blocking collectives, shards(): lax.all_gather(query_nope, 'tp', axis=1, tiled=True)  5.2 us
    all_gather x1, blocking collectives, shards(): lax.all_gather(query_rotary, 'tp', axis=1, tiled=True)  5.19 us
    all_to_all x1, waiting for transfers between devices, shards(): lax.all_to_all(to_pieces(hidden_summary, sp_count, tp_count), ('sp', 'tp'...  2.41 us
    unnamed x22, local copies, waits for them, and re-layouts  2.26 us
  transfers between devices with their start and end apart: 2, of which 2 were waited for; matrix products, arithmetic and copies ran while one was open for 7% of the time, Pallas kernels for 0%

commit v1 on v0

--- a/solution.py
+++ b/solution.py
@@ -79,12 +79,20 @@
         jnp.bfloat16
     )
     moved = (
-        lax.all_to_all(
-            to_pieces(hidden_summary, sp_count, tp_count),
-            ("sp", "tp"),
-            split_axis=0,
-            concat_axis=2,
-            tiled=True,
+        jnp.concatenate(
+            lax.all_to_all(
+                jnp.stack(
+                    jnp.split(
+                        to_pieces(hidden_summary, sp_count, tp_count),
+                        lax.axis_size(("sp", "tp")),
+                        axis=0,
+                    )
+                ),
+                ("sp", "tp"),
+                split_axis=0,
+                concat_axis=0,
+            ),
+            axis=2,
         ),
         lax.all_to_all(
             to_pieces(rotary, sp_count, tp_count),

time: 55.9 us -> 74.4 us (1.33)
  local copies, waits for them, and re-layouts: 4.3 us -> 22.7 us
  waiting for transfers between devices: 2.64 us -> 1.38 us
  matrix products: 2.46 us -> 3.52 us
    unnamed x22 -> x51, local copies, waits for them, and re-layouts: 2.26 us -> 20.8 us
    dot_general x1, matrix products: 0.36 us -> 1.4 us  [shards(): jnp.einsum('shd,chd->shc', query_all, lookup_widening, preferred_element_...]
    all_to_all x1, waiting for transfers between devices: 2.41 us -> 1.38 us  [shards(): lax.all_to_all(jnp.stack(jnp.split(to_pieces(hidden_summary, sp_count, tp...]
  transfers between devices with their start and end apart: 2 -> 2, of which waited for: 2 -> 1; matrix products, arithmetic and copies ran while one was open for 7% -> 32% of each run, Pallas kernels for 0% -> 0%
where the time goes in v1:
time: 74.4 us; the launch traced here: 74.1 us
  blocking collectives  26.7 us (36%)
  local copies, waits for them, and re-layouts  22.7 us (31%)
  starting transfers between devices  13.2 us (18%)
  other arithmetic  4.95 us (7%)
  matrix products  3.52 us (5%)
  between operations  1.57 us (2%)
  waiting for transfers between devices  1.38 us (2%)
    unnamed x51, local copies, waits for them, and re-layouts  20.8 us
    psum x1, blocking collectives, shards(): lax.psum(partial_value.astype(jnp.bfloat16), 'tp').astype(jnp.float32)  10.6 us
    all_to_all x1, starting transfers between devices, shards(): lax.all_to_all(to_pieces(rotary, sp_count, tp_count), ('sp', 'tp'), split...  7.33 us
    all_to_all x1, starting transfers between devices, shards(): lax.all_to_all(jnp.stack(jnp.split(to_pieces(hidden_summary, sp_count, tp...  5.83 us
    unnamed x1, blocking collectives  5.76 us
    all_gather x1, blocking collectives, shards(): lax.all_gather(query_nope, 'tp', axis=1, tiled=True)  5.2 us
    all_gather x1, blocking collectives, shards(): lax.all_gather(query_rotary, 'tp', axis=1, tiled=True)  5.19 us
    reduce_sum x2, other arithmetic, rescaled_lines(): jnp.mean(vector * vector, axis=-1, keepdims=True) + norm_eps  1.81 us
  transfers between devices with their start and end apart: 2, of which 1 were waited for; matrix products, arithmetic and copies ran while one was open for 32% of the time, Pallas kernels for 0%

profile of v1, /device:TPU:0, one launch (start us, length us, event | category | flops | bytes accessed | tf_op | source)
XLA Modules:
  0.0 74.1 jit_solution(17798059621956757741)
XLA Ops:
  0.7 1.7 %fusion = f32[8,32]{1,0:T(8,128)S(1)} fusion(bf16[8,32,2048]{2,1,0:T(8,128)(2,1)} %param.9), kind=kLoop, calls=%fused_computation.2 | loop fusion | flops 1572608 | bytes 1049600 | tf_op jit(solution)/shard_map/reduce_sum | solution.py:18
  2.4 1.5 %fusion.2 = bf16[8,32,2048]{2,1,0:T(8,128)(2,1)S(1)} fusion(bf16[8,32,2048]{2,1,0:T(8,128)(2,1)} %param.9, f32[2048]{0:T(1024)} %param.10, f32[8,32]{1,0:T(8,128)S(1)} %add_rsqrt_fusion), kind=kLoop, calls=%fused_computation.4 | loop fusion | flops 2097152 | bytes 2106368 | tf_op jit(solution)/shard_map/convert_element_type | solution.py:62
  5.0 0.8 %reshape.296 = bf16[32,2,256]{2,1,0:T(2,128)(2,1)} reshape(bf16[32,1,16,32]{3,2,1,0:T(8,128)(2,1)S(1)} %bitcast.252) | data formatting | bytes 65536
  5.8 7.3 %all-to-all-start.1 = ((bf16[32,2,256]{2,1,0:T(2,128)(2,1)}), bf16[32,2,256]{2,1,0:T(2,128)(2,1)S(1)}, u32[]{:S(2)}, u32[]{:S(2)}) async-start(bf16[32,2,256]{2,1,0:T(2,128)(2,1)} %reshape.296), calls=%async_computation.1 | async-start | bytes 65536 | tf_op jit(solution)/shard_map/all_to_all | solution.py:97
  13.1 5.2 %all_gather.7 = bf16[1,16,64]{2,0,1:T(2,128)(2,1)S(1)} all-gather(bf16[1,4,64]{2,0,1:T(2,128)(2,1)S(1)} %copy.221), channel_id=1, replica_groups=mesh['sp'=8,'tp'=4] {'tp'}, dimensions={1}, use_global_device_ids=true | all-gather | bytes 2560 | tf_op jit(solution)/shard_map/all_gather | solution.py:112
  18.3 0.8 %multiply_reduce_fusion = (f32[256]{0:T(256)S(1)}, f32[256,512]{1,0:T(8,128)S(1)}) fusion(bf16[256,2048]{1,0:T(8,128)(2,1)S(1)} %bitcast.215, bf16[2048,512]{1,0:T(8,128)(2,1)S(1)} %copy-done), kind=kOutput, calls=%fused_computation.20 | convolution fusion | flops 537394944 | bytes 3671040 | tf_op jit(solution)/shard_map/dot_general | solution.py:64
  19.4 0.6 constant_dynamic-update-slice_fusion.31
  20.0 0.6 constant_dynamic-update-slice_fusion.30
  21.8 0.6 constant_dynamic-update-slice_fusion.27
  22.4 0.6 constant_dynamic-update-slice_fusion.26
  24.2 0.6 constant_dynamic-update-slice_fusion.23
  26.0 0.6 constant_dynamic-update-slice_fusion.20
  27.8 0.6 constant_dynamic-update-slice_fusion.17
  29.6 0.6 constant_dynamic-update-slice_fusion.14
  31.4 0.6 constant_dynamic-update-slice_fusion.11
  38.6 5.8 %all-to-all-start = ((bf16[32,1,1,32,128]{4,3,2,1,0:T(8,128)(2,1)}), bf16[32,1,1,32,128]{4,3,2,1,0:T(8,128)(2,1)S(1)}, u32[]{:S(2)}, u32[]{:S(2)}) async-start(bf16[32,1,1,32,128]{4,3,2,1,0:T(8,128)(2,1)} %constant_dynamic-update-slice_fusion), calls=%async_computation | async-start | bytes 524288 | tf_op jit(solution)/shard_map/all_to_all | solution.py:83
  45.8 5.2 %all_gather.6 = bf16[1,16,128]{2,0,1:T(2,128)(2,1)S(1)} all-gather(bf16[1,4,128]{2,0,1:T(2,128)(2,1)S(1)} %copy.220), channel_id=1, replica_groups=mesh['sp'=8,'tp'=4] {'tp'}, dimensions={1}, use_global_device_ids=true | all-gather | bytes 5120 | tf_op jit(solution)/shard_map/all_gather | solution.py:111
  51.1 1.4 %fusion.11 = f32[16,1,128]{2,1,0:T(1,128)S(1)} fusion(bf16[128,16,128]{2,1,0:T(8,128)(2,1)} %param.14, bf16[1,16,128]{2,0,1:T(2,128)(2,1)S(1)} %all_gather.6), kind=kOutput, calls=%fused_computation.17 | convolution fusion | flops 524288 | bytes 536576 | tf_op jit(solution)/shard_map/shd,chd->shc/dot_general | solution.py:114
  52.9 0.8 %squeeze.3 = bf16[1,1024,16]{1,2,0:T(8,128)(2,1)} reshape(bf16[32,1,32,16]{2,0,3,1:T(8,128)(2,1)S(1)} %copy.219) | data formatting | bytes 65536 | tf_op jit(solution)/shard_map/squeeze | solution.py:106
  53.6 1.4 %all-to-all-done = bf16[32,1,1,32,128]{4,3,2,1,0:T(8,128)(2,1)S(1)} async-done(((bf16[32,1,1,32,128]{4,3,2,1,0:T(8,128)(2,1)}), bf16[32,1,1,32,128]{4,3,2,1,0:T(8,128)(2,1)S(1)}, u32[]{:S(2)}, u32[]{:S(2)}) %all-to-all-start) | async-done | bytes 262176 | tf_op jit(solution)/shard_map/all_to_all | solution.py:83
  55.4 10.6 %psum.7 = bf16[1,16,1024]{2,1,0:T(8,128)(2,1)S(1)} all-reduce(bf16[1,16,1024]{2,1,0:T(8,128)(2,1)S(1)} %fusion.7), channel_id=1, replica_groups=mesh['sp'=8,'tp'=4] {'tp'}, use_global_device_ids=true, to_apply=%region_2.0 | all-reduce | flops 16384 | bytes 65536 | tf_op jit(solution)/shard_map/psum | solution.py:126
  66.8 5.8 %all-reduce = f32[16,1,128]{2,0,1:T(8,128)S(1)} all-reduce(f32[16,1,128]{2,0,1:T(8,128)S(1)} %bitcast.254), channel_id=2, replica_groups=mesh['sp'=8,'tp'=4] {'tp'}, use_global_device_ids=true, to_apply=%region_5.0.clone | all-reduce | flops 2048 | bytes 16384
  72.7 0.6 multiply_convert_fusion.1
  73.4 0.7 copy.271
  (69 shorter events, 17.5 us)
Async XLA Ops:
  0.6 17.7 %copy-start = (bf16[2048,512]{1,0:T(8,128)(2,1)S(1)}, bf16[2048,512]{1,0:T(8,128)(2,1)}, u32[]{:S(2)}) copy-start(bf16[2048,512]{1,0:T(8,128)(2,1)} %param.11) | copy-start | bytes 6291460
  0.6 3.3 %copy-start.1 = (bf16[2048,64]{0,1:T(8,128)(2,1)S(1)}, bf16[2048,64]{0,1:T(8,128)(2,1)}, u32[]{:S(2)}) copy-start(bf16[2048,64]{0,1:T(8,128)(2,1)} %param.12) | copy-start | bytes 786436
  2.4 10.7 %copy-start.3 = (bf16[1,4,64]{2,1,0:T(4,128)(2,1)S(1)}, bf16[1,4,64]{2,1,0:T(4,128)(2,1)}, u32[]{:S(2)}) copy-start(bf16[1,4,64]{2,1,0:T(4,128)(2,1)} %param.17) | copy-start | bytes 1540
  5.0 14.2 %copy-start.2 = (f32[512]{0:T(512)S(1)}, f32[512]{0:T(512)}, u32[]{:S(2)}) copy-start(f32[512]{0:T(512)} %param.13) | copy-start | bytes 6148
  5.8 32.9 %all-to-all-start.1 = ((bf16[32,2,256]{2,1,0:T(2,128)(2,1)}), bf16[32,2,256]{2,1,0:T(2,128)(2,1)S(1)}, u32[]{:S(2)}, u32[]{:S(2)}) async-start(bf16[32,2,256]{2,1,0:T(2,128)(2,1)} %reshape.296), calls=%async_computation.1 | async-start | bytes 65536 | tf_op jit(solution)/shard_map/all_to_all | solution.py:97
  19.1 25.4 %copy-start.4 = (bf16[1,4,128]{2,1,0:T(4,128)(2,1)S(1)}, bf16[1,4,128]{2,1,0:T(4,128)(2,1)}, u32[]{:S(2)}) copy-start(bf16[1,4,128]{2,1,0:T(4,128)(2,1)} %param.16) | copy-start | bytes 3076
  19.1 25.4 %copy-start.6 = (u32[32]{0:T(128)S(1)}, u32[32]{0:T(128)}, u32[]{:S(2)}) copy-start(u32[32]{0:T(128)} %constant.54) | copy-start | bytes 388
  19.4 47.2 %copy-start.5 = (bf16[128,16,128]{2,1,0:T(8,128)(2,1)S(1)}, bf16[128,16,128]{2,1,0:T(8,128)(2,1)}, u32[]{:S(2)}) copy-start(bf16[128,16,128]{2,1,0:T(8,128)(2,1)} %param.15) | copy-start | bytes 1572868
  38.6 16.4 %all-to-all-start = ((bf16[32,1,1,32,128]{4,3,2,1,0:T(8,128)(2,1)}), bf16[32,1,1,32,128]{4,3,2,1,0:T(8,128)(2,1)S(1)}, u32[]{:S(2)}, u32[]{:S(2)}) async-start(bf16[32,1,1,32,128]{4,3,2,1,0:T(8,128)(2,1)} %constant_dynamic-update-slice_fusion), calls=%async_computation | async-start | bytes 524288 | tf_op jit(solution)/shard_map/all_to_all | solution.py:83
